TPU v7x, 32 devices: a whole 2x2x4 slice. The times are simulated.
32 devices in a mesh: sp: 8 (over z, y), tp: 4 (over x, core).
Axes of the slice: x: 2, y: 2, z: 4, core: 2. Of those that a mesh axis runs over, the one named last changes fastest.
Arguments:
- conv_input: bfloat16 [2048, 2048], P('sp', 'tp'), may hold values from -6 to 6
- gate_branch: bfloat16 [2048, 2048], P('sp', 'tp'), may hold values from -6 to 6
- conv_taps: float32 [4, 2048], P(None, 'tp'), may hold values from -3 to 3
- narrow_maps: bfloat16 [2, 8, 128, 128], P(None, 'tp'), may hold values from -0.5 to 0.5
- wide_maps: bfloat16 [2, 4, 256, 256], P(None, 'tp'), may hold values from -0.375 to 0.375
- decay_param: float32 [2048], P('tp'), may hold values from 4.5 to 20
- decay_shift: float32 [2048, 2048], P('sp', 'tp'), may hold values from -0.75 to 0
- mixer_out: bfloat16 [2048, 2048], P('tp'), may hold values from -0.125 to 0.125
- stream: bfloat16 [2048, 2048], P(('sp', 'tp')), may hold values from -6 to 6
- norm_gain: float32 [2048], replicated, may hold values from 0.1 to 1.9
- routes: int32 [2048, 4], P('sp'), may hold values from 0 to 7, all different within a row; in each aligned block of 64 rows (0 to 63, 64 to 127, ...) at most 64 rows name the same one
- route_weights: float32 [2048, 4], P('sp'), may hold values from 0.05 to 0.5
- expert_gate: bfloat16 [8, 2048, 2048], P('sp', None, 'tp'), may hold values from -1 to 1
- expert_up: bfloat16 [8, 2048, 2048], P('sp', None, 'tp'), may hold values from -1 to 1
- expert_down: bfloat16 [8, 2048, 2048], P('sp', 'tp'), may hold values from -0.015625 to 0.015625
Outputs:
- layer_out: bfloat16 [2048, 2048], P(('sp', 'tp'))
Inputs may be any that keep to these rules, and one draw needn't show every extreme that they name: `routes`: each row names 4 different experts. In each aligned block of 64 rows no expert is named more than 64 times, and in every draw some expert is named exactly 64 times in some block.
All inputs are finite; a program needn't handle non-finite values.
Results may differ from a plain program's by a relative error of at most 0.015.
Values may be sent and summed in bfloat16 or wider, within the bound.
A program may use at most 128 MiB of HBM per device.

v0:
```python
import jax
import jax.numpy as jnp
from jax import lax
from jax.sharding import PartitionSpec as P

NORM_EPSILON = 1e-06
CLAMP_LIMIT = 7.0
GATE_SLOPE = 1.702
DECAY_SCALE = 8.0


def shifted(block, axis, distance):
    devices = range(lax.axis_size(axis))
    route = [(i - distance, i) for i in devices if i - distance in devices]
    return lax.ppermute(block, axis, route)


def prefix(value, axis, join, neutral):
    count, mine = (lax.axis_size(axis), lax.axis_index(axis))
    pieces = jax.tree.map(lambda part: lax.all_gather(part, axis), value)
    so_far = jax.tree.map(
        lambda part, zero: jnp.full_like(part, 0) + jnp.asarray(zero, part.dtype), value, neutral
    )

    def lap(position, so_far):
        longer = join(so_far, jax.tree.map(lambda part: part[position], pieces))
        return jax.tree.map(lambda new, old: jnp.where(position < mine, new, old), longer, so_far)

    return lax.fori_loop(0, count - 1, lap, so_far)


def combine_steps(earlier, later):
    return (earlier[0] * later[0], later[0] * earlier[1] + later[1])


def head_maps(convolved, narrow_maps, wide_maps):
    seq_rows = convolved.shape[0]
    wide_count = wide_maps.shape[1]
    wide_size = wide_maps.shape[2]
    narrow_size = narrow_maps.shape[2]
    segments = convolved.reshape(seq_rows, wide_count, 2 * narrow_size + wide_size)
    narrow = segments[:, :, : 2 * narrow_size].reshape(seq_rows, 2 * wide_count, narrow_size)
    wide_part = segments[:, :, 2 * narrow_size :]
    narrow_pre = jnp.einsum(
        "rhi,mhio->mrho", narrow, narrow_maps, preferred_element_type=jnp.float32
    )
    wide_pre = jnp.einsum(
        "rhi,mhio->mrho", wide_part, wide_maps, preferred_element_type=jnp.float32
    )
    narrow_pre = narrow_pre.reshape(2, seq_rows, wide_count, 2 * narrow_size)
    return jnp.concatenate([narrow_pre, wide_pre], axis=3).reshape(2, seq_rows, convolved.shape[1])


def clamp_units(gate_pre, up_pre):
    clamped = jnp.minimum(gate_pre, CLAMP_LIMIT)
    upper = jnp.clip(up_pre, -CLAMP_LIMIT, CLAMP_LIMIT)
    return (upper + 1.0) * clamped * jax.nn.sigmoid(GATE_SLOPE * clamped)


def slot_ranks(flat_routes, expert_total):
    onehot = (
        flat_routes[:, :, None] == jnp.arange(expert_total, dtype=jnp.int32)[None, None, :]
    ).astype(jnp.int32)
    return jnp.sum(jnp.cumsum(onehot, axis=1) * onehot, axis=2) - 1


def take_rows(source_rows, slot_source):
    filled = slot_source >= 0
    picked = source_rows[jnp.maximum(slot_source, 0)]
    return jnp.where(filled[:, None], picked, jnp.zeros_like(picked))


def expert_work(arrived, expert_gate, expert_up, expert_down):
    local_experts = expert_gate.shape[0]
    buffer_shape = arrived.shape
    grouped = arrived.reshape(
        buffer_shape[0] // local_experts,
        local_experts,
        buffer_shape[1] * buffer_shape[2],
        buffer_shape[3],
    )
    gate_pre = jnp.einsum(
        "sxcd,xdf->sxcf", grouped, expert_gate, preferred_element_type=jnp.float32
    )
    up_pre = jnp.einsum("sxcd,xdf->sxcf", grouped, expert_up, preferred_element_type=jnp.float32)
    activation = clamp_units(gate_pre, up_pre).astype(jnp.bfloat16)
    partial_value = jnp.einsum(
        "sxcf,xfd->sxcd", activation, expert_down, preferred_element_type=jnp.float32
    )
    return partial_value.reshape(buffer_shape)


def shards(
    conv_input,
    gate_branch,
    conv_taps,
    narrow_maps,
    wide_maps,
    decay_param,
    decay_shift,
    mixer_out,
    stream,
    norm_gain,
    routes,
    route_weights,
    expert_gate,
    expert_up,
    expert_down,
):
    seq_rows, channels = conv_input.shape
    tap_count = conv_taps.shape[0]
    earlier = shifted(conv_input[seq_rows - tap_count + 1 :], "sp", 1)
    padded = jnp.concatenate([earlier, conv_input], axis=0).astype(jnp.float32)
    convolved = jnp.zeros((seq_rows, channels), jnp.float32)
    for offset in range(tap_count):
        convolved = convolved + padded[offset : offset + seq_rows] * conv_taps[offset]
    convolved = convolved.astype(jnp.bfloat16)
    gate_pre = head_maps(convolved, narrow_maps, wide_maps)
    log_decay = (
        -DECAY_SCALE * jax.nn.sigmoid(gate_pre[0]) * jax.nn.softplus(-decay_param) + decay_shift
    )
    driving = (
        jnp.sqrt(-jnp.expm1(2.0 * log_decay))
        * jax.nn.sigmoid(gate_pre[1])
        * convolved.astype(jnp.float32)
    )
    identity = (jnp.ones((channels,), jnp.float32), jnp.zeros((channels,), jnp.float32))
    factors, local_state = lax.associative_scan(
        combine_steps, (jnp.exp(log_decay), driving), axis=0
    )
    carried = prefix((factors[-1], local_state[-1]), "sp", combine_steps, identity)
    recurrent = local_state + factors * carried[1]
    gated_rows = (recurrent * jax.nn.gelu(gate_branch.astype(jnp.float32))).astype(jnp.bfloat16)
    tp_count = lax.axis_size("tp")
    tok_local = seq_rows // tp_count
    mixer_sum = lax.psum_scatter(
        jnp.dot(gated_rows, mixer_out, preferred_element_type=jnp.float32).astype(jnp.bfloat16),
        "tp",
        scatter_dimension=0,
        tiled=True,
    ).astype(jnp.float32)
    hidden_f = stream.astype(jnp.float32) + mixer_sum
    hidden = hidden_f.astype(jnp.bfloat16)
    hidden_f = hidden.astype(jnp.float32)
    normed = (
        hidden_f
        * lax.rsqrt(jnp.mean(hidden_f * hidden_f, axis=-1, keepdims=True) + NORM_EPSILON)
        * norm_gain
    ).astype(jnp.bfloat16)
    model_width = normed.shape[1]
    top_count = routes.shape[1]
    expert_total = expert_gate.shape[0] * lax.axis_size("sp")
    capacity = max(2, 2 * tok_local * top_count // expert_total)
    own_index = lax.axis_index("tp")
    assignments = tok_local * top_count
    own_rows = lax.dynamic_slice_in_dim(routes, own_index * tok_local, tok_local, 0)
    own_routes = own_rows.reshape(assignments)
    own_ranks = slot_ranks(own_routes[None, :], expert_total)[0]
    source = jnp.arange(assignments, dtype=jnp.int32) // top_count
    slot_source = (
        jnp.full((expert_total * capacity,), -1, jnp.int32)
        .at[own_routes * capacity + own_ranks]
        .set(source)
    )
    outgoing = take_rows(normed, slot_source).reshape(expert_total, 1, capacity, model_width)
    partial_value = expert_work(
        lax.all_gather(
            lax.all_to_all(outgoing, "sp", split_axis=0, concat_axis=0, tiled=True),
            "tp",
            axis=1,
            tiled=True,
        ),
        expert_gate,
        expert_up,
        expert_down,
    )
    summed = lax.psum_scatter(
        partial_value.astype(jnp.bfloat16), "tp", scatter_dimension=1, tiled=True
    )
    returned = lax.all_to_all(summed, "sp", split_axis=0, concat_axis=0, tiled=True)
    own_slots = own_routes * capacity + own_ranks
    picked = returned.reshape(expert_total * capacity, model_width)[own_slots]
    own_weights = lax.dynamic_slice_in_dim(route_weights, own_index * tok_local, tok_local, 0)
    combined = jnp.sum(
        picked.reshape(tok_local, top_count, model_width).astype(jnp.float32)
        * own_weights[:, :, None],
        axis=1,
    )
    return (hidden_f + combined).astype(jnp.bfloat16)


def solution(mesh):
    placed = (
        P("sp", "tp"),
        P("sp", "tp"),
        P(None, "tp"),
        P(None, "tp", None, None),
        P(None, "tp", None, None),
        P("tp"),
        P("sp", "tp"),
        P("tp", None),
        P(("sp", "tp"), None),
        P(),
        P("sp", None),
        P("sp", None),
        P("sp", None, "tp"),
        P("sp", None, "tp"),
        P("sp", "tp", None),
    )
    return jax.shard_map(
        shards, mesh=mesh, in_specs=placed, out_specs=P(("sp", "tp"), None), check_vma=False
    )
```

profile of v0, /device:TPU:24, one launch (start us, length us, event | category | flops | bytes accessed | tf_op | source)
XLA Modules:
  0.0 558.1 jit_solution(4091853979473542298)
XLA Ops:
  7.4 3.4 collective-permute-start
  17.7 1.9 fusion.28
  25.3 2.0 multiply_add_fusion
  31.9 1.8 multiply_add_fusion.1
  101.4 1.7 pad.113
  103.3 1.9 fusion.35
  107.7 22.5 %all-gather.1 = f32[8,1,512]{2,1,0:T(1,128)S(1)} all-gather(f32[1,1,512]{2,1,0:T(1,128)S(1)} %add_bitcast_fusion), channel_id=1, replica_groups=mesh['sp'=8,'tp'=4] {'sp'}, dimensions={0}, use_global_device_ids=true | all-gather | bytes 18432 | tf_op jit(solution)/shard_map/all_gather | solution.py:20
  130.2 1.7 pad.129
  132.9 1.7 pad.128
  135.4 26.1 %all-gather = f32[8,1,512]{2,1,0:T(1,128)S(1)} all-gather(f32[1,1,512]{2,1,0:T(1,128)S(1)} %add_bitcast_fusion.1), channel_id=1, replica_groups=mesh['sp'=8,'tp'=4] {'sp'}, dimensions={0}, use_global_device_ids=true | all-gather | bytes 18432 | tf_op jit(solution)/shard_map/all_gather | solution.py:20
  161.9 4.1 convolution_convert_fusion.1
  169.1 22.9 %reduce-scatter.5.cloned.1.call-done = bf16[64,2048]{1,0:T(8,128)(2,1)} async-done(((bf16[256,2048]{1,0:T(8,128)(2,1)}), bf16[64,2048]{1,0:T(8,128)(2,1)}) %reduce-scatter.5.cloned.1.call-update) | async-done | bytes 262160 | tf_op jit(solution)/shard_map/reduce_scatter | solution.py:136
  194.2 3.3 gather_fusion
  197.5 1.8 broadcast_select_fusion
  199.3 51.3 %all_to_all.10 = bf16[8,1,64,2048]{3,2,1,0:T(8,128)(2,1)} all-to-all(bf16[8,1,64,2048]{3,2,1,0:T(8,128)(2,1)S(1)} %broadcast_select_fusion), channel_id=1, replica_groups=mesh['sp'=8,'tp'=4] {'sp'}, dimensions={0} | all-to-all | bytes 4194304 | tf_op jit(solution)/shard_map/all_to_all | solution.py:168
  250.8 58.5 %all-gather.4.cloned.1.call-done = bf16[8,4,64,2048]{3,2,1,0:T(8,128)(2,1)} async-done(((bf16[8,1,64,2048]{3,2,1,0:T(8,128)(2,1)}), bf16[8,4,64,2048]{3,2,1,0:T(8,128)(2,1)}) %all-gather.4.cloned.1.call-update) | async-done | bytes 8388624 | tf_op jit(solution)/shard_map/all_gather | solution.py:167
  309.3 10.4 %fusion.2 = f32[8,256,512]{2,1,0:T(8,128)} fusion(bf16[8,256,2048]{2,1,0:T(8,128)(2,1)} %bitcast.131, bf16[1,2048,512]{2,1,0:T(8,128)(2,1)} %param.30), kind=kOutput, calls=%fused_computation.11 | convolution fusion | flops 4294967296 | bytes 14680064 | tf_op jit(solution)/shard_map/sxcd,xdf->sxcf/dot_general | solution.py:85
  319.7 15.3 %convolution_convert_fusion = bf16[8,256,2048]{2,1,0:T(8,128)(2,1)} fusion(bf16[1,512,2048]{2,1,0:T(8,128)(2,1)S(1)} %copy-done, f32[8,256,512]{2,1,0:T(8,128)} %fusion.2, bf16[8,256,2048]{2,1,0:T(8,128)(2,1)} %bitcast.132, bf16[1,2048,512]{2,1,0:T(8,128)(2,1)} %param.29), kind=kOutput, calls=%fused_computation.6 | convolution fusion | flops 8604614656 | bytes 25165824 | tf_op jit(solution)/shard_map/sxcf,xfd->sxcd/dot_general | solution.py:87
  336.2 151.8 %all-reduce.35.cloned.1.call-done = bf16[8,4,64,2048]{3,2,1,0:T(8,128)(2,1)} async-done(((bf16[8,4,64,2048]{3,2,1,0:T(8,128)(2,1)}), bf16[8,4,64,2048]{3,2,1,0:T(8,128)(2,1)}) %all-reduce.35.cloned.1.call-update) | async-done | bytes 8388624
  488.0 3.9 constant_dynamic-slice_fusion.2
  491.9 6.1 %all-to-all-start.1 = ((bf16[8,1,64,2048]{3,2,1,0:T(8,128)(2,1)}), bf16[8,1,64,2048]{3,2,1,0:T(8,128)(2,1)S(1)}, u32[]{:S(2)}, u32[]{:S(2)}) async-start(bf16[8,1,64,2048]{3,2,1,0:T(8,128)(2,1)} %constant_dynamic-slice_fusion.2), calls=%async_computation.2 | async-start | bytes 4194304 | tf_op jit(solution)/shard_map/all_to_all | solution.py:180
  498.2 46.2 %all-to-all-done.1 = bf16[8,1,64,2048]{3,2,1,0:T(8,128)(2,1)S(1)} async-done(((bf16[8,1,64,2048]{3,2,1,0:T(8,128)(2,1)}), bf16[8,1,64,2048]{3,2,1,0:T(8,128)(2,1)S(1)}, u32[]{:S(2)}, u32[]{:S(2)}) %all-to-all-start.1) | async-done | bytes 2097184 | tf_op jit(solution)/shard_map/all_to_all | solution.py:180
  545.8 1.7 reshape.277
  547.5 3.2 multiply_reduce_fusion
  (223 shorter events, 99.3 us)
Async XLA Ops:
  6.5 313.2 %copy-start = (bf16[1,512,2048]{2,1,0:T(8,128)(2,1)S(1)}, bf16[1,512,2048]{2,1,0:T(8,128)(2,1)}, u32[]{:S(2)}) copy-start(bf16[1,512,2048]{2,1,0:T(8,128)(2,1)} %param.31) | copy-start | bytes 6291460
  6.5 8.7 %copy-start.10 = (bf16[2,2,128,128]{3,2,1,0:T(8,128)(2,1)S(1)}, bf16[2,2,128,128]{3,2,1,0:T(8,128)(2,1)}, u32[]{:S(2)}) copy-start(bf16[2,2,128,128]{3,2,1,0:T(8,128)(2,1)} %param.20) | copy-start | bytes 393220
  6.5 185.4 %reduce-scatter.5.cloned.1.call-start = ((), (), s32[]{:S(2)}) async-start(), calls=%async_computation.3 | async-start | bytes 1310720 | tf_op jit(solution)/shard_map/reduce_scatter | solution.py:136
  7.4 6.4 %collective-permute-start = (bf16[3,512]{1,0:T(4,128)(2,1)S(1)}, bf16[3,512]{1,0:T(4,128)(2,1)S(1)}, u32[]{:S(2)}, u32[]{:S(2)}) collective-permute-start(bf16[3,512]{1,0:T(4,128)(2,1)S(1)} %slice.283), channel_id=1, source_target_pairs={{0,4},{4,8},{8,12},{12,16},{16,20},{20,24},{24,28},{1,5},{5,9},{9,... | collective-permute-start | bytes 9224 | tf_op jit(solution)/shard_map/ppermute | solution.py:15
  19.8 72.3 %copy-start.2 = (f32[256,512]{1,0:T(8,128)}, f32[256,512]{1,0:T(8,128)S(1)}, u32[]{:S(2)}) copy-start(f32[256,512]{1,0:T(8,128)S(1)} %exp.21) | copy-start | bytes 1572868
  89.2 10.2 %copy-start.16 = (f32[1,512]{1,0:T(1,128)S(1)}, f32[1,512]{1,0:T(1,128)}, u32[]{:S(2)}) copy-start(f32[1,512]{1,0:T(1,128)} %slice.415) | copy-start | bytes 6148
  89.2 11.0 %copy-start.8 = (f32[31,512]{1,0:T(8,128)S(1)}, f32[31,512]{1,0:T(8,128)}, u32[]{:S(2)}) copy-start(f32[31,512]{1,0:T(8,128)} %slice.309) | copy-start | bytes 190468
  90.6 10.5 %copy-start.15 = (f32[1,512]{1,0:T(1,128)S(1)}, f32[1,512]{1,0:T(1,128)}, u32[]{:S(2)}) copy-start(f32[1,512]{1,0:T(1,128)} %slice.388) | copy-start | bytes 6148
  92.0 8.2 %copy-start.9 = (f32[31,512]{1,0:T(8,128)S(1)}, f32[31,512]{1,0:T(8,128)}, u32[]{:S(2)}) copy-start(f32[31,512]{1,0:T(8,128)} %slice.350) | copy-start | bytes 190468
  96.4 4.8 copy-start.7
  101.1 2.0 copy-start.13
  103.3 28.7 %slice-start = ((f32[256,512]{1,0:T(8,128)}), f32[1,512]{1,0:T(1,128)S(1)}, s32[]{:S(2)}) async-start(f32[256,512]{1,0:T(8,128)} %copy-done.2), calls=%async_computation.6 | async-start | bytes 4096 | tf_op jit(solution)/shard_map/slice | solution.py:128
  105.2 56.3 %copy-start.11 = (f32[512]{0:T(512)S(1)}, f32[512]{0:T(512)}, u32[]{:S(2)}) copy-start(f32[512]{0:T(512)} %custom-call) | copy-start | bytes 6148
  105.2 56.7 %copy-start.5 = (f32[256,512]{1,0:T(8,128)S(1)}, f32[256,512]{1,0:T(8,128)}, u32[]{:S(2)}) copy-start(f32[256,512]{1,0:T(8,128)} %pad.113) | copy-start | bytes 1572868
  107.0 54.9 %copy-start.6 = (f32[256,512]{1,0:T(8,128)}, f32[256,512]{1,0:T(8,128)S(1)}, u32[]{:S(2)}) copy-start(f32[256,512]{1,0:T(8,128)S(1)} %pad.112) | copy-start | bytes 1572868
  161.9 4.2 copy-start.17
  161.9 30.0 %copy-start.3 = (bf16[64,2048]{1,0:T(8,128)(2,1)S(1)}, bf16[64,2048]{1,0:T(8,128)(2,1)}, u32[]{:S(2)}) copy-start(bf16[64,2048]{1,0:T(8,128)(2,1)} %param.25) | copy-start | bytes 786436
  161.9 31.2 %copy-start.12 = (f32[2048]{0:T(1024)S(1)}, f32[2048]{0:T(1024)}, u32[]{:S(2)}) copy-start(f32[2048]{0:T(1024)} %param.26) | copy-start | bytes 24580
  166.0 143.2 %all-gather.4.cloned.1.call-start = ((), (), s32[]{:S(2)}) async-start(), calls=%async_computation.4 | async-start | bytes 10485760 | tf_op jit(solution)/shard_map/all_gather | solution.py:167
  250.6 237.5 %all-reduce.35.cloned.1.call-start = ((), (), s32[]{:S(2)}) async-start(), calls=%async_computation.5 | async-start | bytes 16777216
  491.9 6.1 %copy-start.18 = (f32[256,4]{0,1:T(4,128)S(1)}, f32[256,4]{0,1:T(4,128)}, u32[]{:S(2)}) copy-start(f32[256,4]{0,1:T(4,128)} %param.28) | copy-start | bytes 12292
  491.9 52.5 %all-to-all-start.1 = ((bf16[8,1,64,2048]{3,2,1,0:T(8,128)(2,1)}), bf16[8,1,64,2048]{3,2,1,0:T(8,128)(2,1)S(1)}, u32[]{:S(2)}, u32[]{:S(2)}) async-start(bf16[8,1,64,2048]{3,2,1,0:T(8,128)(2,1)} %constant_dynamic-slice_fusion.2), calls=%async_computation.2 | async-start | bytes 4194304 | tf_op jit(solution)/shard_map/all_to_all | solution.py:180
  545.8 5.8 %copy-start.1 = (bf16[1,512,2048]{2,1,0:T(8,128)(2,1)S(1)}, bf16[1,512,2048]{2,1,0:T(8,128)(2,1)}, u32[]{:S(2)}) copy-start(bf16[1,512,2048]{2,1,0:T(8,128)(2,1)} %param.31) | copy-start | bytes 6291460
  547.5 3.2 copy-start.4
  (2 other events, 2.5 us)
Sparse Core Ops, SparseCore 0:
  166.2 25.7 reduce-scatter.4
  250.7 58.5 all-gather.3
  335.1 152.8 all-reduce.34
where the time goes:
time: 564 us; the launch traced here: 558 us
  waiting for transfers between devices  281 us (50%)
  blocking collectives  99.9 us (18%)
  local copies, waits for them, and re-layouts  84.7 us (15%)
  other arithmetic  37.6 us (7%)
  matrix products  31.2 us (6%)
  between operations  13.8 us (2%)
  starting transfers between devices  9.82 us (2%)
    unnamed x4, waiting for transfers between devices  152 us
    slice x53, local copies, waits for them, and re-layouts, shards(): lax.associative_scan(combine_steps, (jnp.exp(log_decay), driving), axis=0)  60 us
    all_gather x1, waiting for transfers between devices, shards(): lax.all_gather(lax.all_to_all(outgoing, 'sp', split_axis=0, concat_axis=0...  58.5 us
    all_to_all x1, blocking collectives, shards(): lax.all_to_all(outgoing, 'sp', split_axis=0, concat_axis=0, tiled=True)  51.3 us
    all_gather x2, blocking collectives, prefix(): pieces = jax.tree.map(lambda part: lax.all_gather(part, axis), value)  48.6 us
    all_to_all x1, waiting for transfers between devices, shards(): lax.all_to_all(summed, 'sp', split_axis=0, concat_axis=0, tiled=True)  46.2 us
    reduce_scatter x1, waiting for transfers between devices, shards(): lax.psum_scatter(jnp.dot(gated_rows, mixer_out, preferred_element_type=jn...  22.9 us
    dot_general x1, matrix products, expert_work(): jnp.einsum('sxcf,xfd->sxcd', activation, expert_down, preferred_element_t...  15.3 us
  transfers between devices with their start and end apart: 5, of which 5 were waited for; matrix products, arithmetic and copies ran while one was open for 1% of the time, Pallas kernels for 0%

commit v1 on v0

--- a/solution.py
+++ b/solution.py
@@ -1,6 +1,10 @@
+import functools
+
 import jax
 import jax.numpy as jnp
 from jax import lax
+from jax.experimental import pallas as pl
+from jax.experimental.pallas import tpu as pltpu
 from jax.sharding import PartitionSpec as P
 
 NORM_EPSILON = 1e-06
@@ -13,42 +17,6 @@
     devices = range(lax.axis_size(axis))
     route = [(i - distance, i) for i in devices if i - distance in devices]
     return lax.ppermute(block, axis, route)
-
-
-def prefix(value, axis, join, neutral):
-    count, mine = (lax.axis_size(axis), lax.axis_index(axis))
-    pieces = jax.tree.map(lambda part: lax.all_gather(part, axis), value)
-    so_far = jax.tree.map(
-        lambda part, zero: jnp.full_like(part, 0) + jnp.asarray(zero, part.dtype), value, neutral
-    )
-
-    def lap(position, so_far):
-        longer = join(so_far, jax.tree.map(lambda part: part[position], pieces))
-        return jax.tree.map(lambda new, old: jnp.where(position < mine, new, old), longer, so_far)
-
-    return lax.fori_loop(0, count - 1, lap, so_far)
-
-
-def combine_steps(earlier, later):
-    return (earlier[0] * later[0], later[0] * earlier[1] + later[1])
-
-
-def head_maps(convolved, narrow_maps, wide_maps):
-    seq_rows = convolved.shape[0]
-    wide_count = wide_maps.shape[1]
-    wide_size = wide_maps.shape[2]
-    narrow_size = narrow_maps.shape[2]
-    segments = convolved.reshape(seq_rows, wide_count, 2 * narrow_size + wide_size)
-    narrow = segments[:, :, : 2 * narrow_size].reshape(seq_rows, 2 * wide_count, narrow_size)
-    wide_part = segments[:, :, 2 * narrow_size :]
-    narrow_pre = jnp.einsum(
-        "rhi,mhio->mrho", narrow, narrow_maps, preferred_element_type=jnp.float32
-    )
-    wide_pre = jnp.einsum(
-        "rhi,mhio->mrho", wide_part, wide_maps, preferred_element_type=jnp.float32
-    )
-    narrow_pre = narrow_pre.reshape(2, seq_rows, wide_count, 2 * narrow_size)
-    return jnp.concatenate([narrow_pre, wide_pre], axis=3).reshape(2, seq_rows, convolved.shape[1])
 
 
 def clamp_units(gate_pre, up_pre):
@@ -88,6 +56,337 @@
         "sxcf,xfd->sxcd", activation, expert_down, preferred_element_type=jnp.float32
     )
     return partial_value.reshape(buffer_shape)
+
+
+LANES = 128
+SUBLANES = 8
+DX, DY, DC = 1, 2, 4
+SERIES_LIMIT = 0.05
+
+
+def mix_kernel(
+    head_ref, conv_ref, taps_ref, narrow_ref, wide_ref, soft_ref, shift_ref,
+    factor_ref, state_ref, padded, log_keep, drive_keep,
+):
+    rows, channels = conv_ref.shape
+    taps = taps_ref.shape[0]
+    padded[0:SUBLANES, :] = head_ref[...]
+    padded[SUBLANES:, :] = conv_ref[...].astype(jnp.float32)
+    total = jnp.zeros((rows, channels), jnp.float32)
+    for k in range(taps):
+        total = total + padded[pl.ds(SUBLANES - taps + 1 + k, rows), :] * taps_ref[k : k + 1, :]
+    convolved = total.astype(jnp.bfloat16)
+    narrow_size, wide_size = narrow_ref.shape[2], wide_ref.shape[2]
+    spans = []
+    for j in range(wide_ref.shape[1]):
+        base = j * (2 * narrow_size + wide_size)
+        spans.append((base, narrow_size, narrow_ref, 2 * j))
+        spans.append((base + narrow_size, narrow_size, narrow_ref, 2 * j + 1))
+        spans.append((base + 2 * narrow_size, wide_size, wide_ref, j))
+    for start, size, maps, head in spans:
+        piece = convolved[:, start : start + size]
+        decay_pre = jnp.dot(piece, maps[0, head], preferred_element_type=jnp.float32)
+        input_pre = jnp.dot(piece, maps[1, head], preferred_element_type=jnp.float32)
+        cols = slice(start, start + size)
+        log_decay = (
+            -DECAY_SCALE * jax.nn.sigmoid(decay_pre) * soft_ref[:, cols] + shift_ref[:, cols]
+        )
+        decay = jnp.exp(log_decay)
+        y = 2.0 * log_decay
+        series = -y * (1.0 + y * (0.5 + y * (1.0 / 6.0 + y * (1.0 / 24.0 + y * (1.0 / 120.0)))))
+        lost = jnp.where(y > -SERIES_LIMIT, series, 1.0 - decay * decay)
+        log_keep[:, cols] = decay
+        drive_keep[:, cols] = (
+            jnp.sqrt(lost) * jax.nn.sigmoid(input_pre) * piece.astype(jnp.float32)
+        )
+    row_id = lax.broadcasted_iota(jnp.int32, (SUBLANES, channels), 0)
+
+    def tile(i, carry):
+        product, state = carry
+        at = pl.ds(pl.multiple_of(i * SUBLANES, SUBLANES), SUBLANES)
+        a, b = log_keep[at, :], drive_keep[at, :]
+        step = 1
+        while step < SUBLANES:
+            inside = row_id >= step
+            a_before = jnp.where(inside, pltpu.roll(a, step, 0), 1.0)
+            b_before = jnp.where(inside, pltpu.roll(b, step, 0), 0.0)
+            b = a * b_before + b
+            a = a * a_before
+            step *= 2
+        b = b + a * state
+        a = a * product
+        factor_ref[at, :] = a
+        state_ref[at, :] = b
+        last = slice(SUBLANES - 1, SUBLANES)
+        return (a[last, :], b[last, :])
+
+    lax.fori_loop(
+        0,
+        rows // SUBLANES,
+        tile,
+        (jnp.ones((1, channels), jnp.float32), jnp.zeros((1, channels), jnp.float32)),
+    )
+
+
+def mix_local(head, conv_input, conv_taps, narrow_maps, wide_maps, soft, decay_shift):
+    shape = conv_input.shape
+    flat = jax.ShapeDtypeStruct(shape, jnp.float32)
+    return pl.pallas_call(
+        mix_kernel,
+        out_shape=(flat, flat),
+        in_specs=[pl.BlockSpec(memory_space=pltpu.VMEM)] * 7,
+        out_specs=(pl.BlockSpec(memory_space=pltpu.VMEM),) * 2,
+        scratch_shapes=[
+            pltpu.VMEM((shape[0] + SUBLANES, shape[1]), jnp.float32),
+            pltpu.VMEM(shape, jnp.float32),
+            pltpu.VMEM(shape, jnp.float32),
+        ],
+        compiler_params=pltpu.CompilerParams(vmem_limit_bytes=32 * 1024 * 1024),
+    )(head, conv_input, conv_taps, narrow_maps, wide_maps, soft, decay_shift)
+
+
+def moe_kernel(
+    depth, ext_ref, hid_ref, gate_hbm, up_hbm, down_hbm, out_ref,
+    xs, part, from_core, from_y, from_x, last_x, last_y, from_z, gate_w, up_w, down_w,
+    load_sem, z_send, z_recv, g_send, g_recv, r_send, r_recv, e_send, e_recv,
+):
+    rows, width = hid_ref.shape
+    half = width // 2
+    wide = xs.shape[-1]
+    sp, tp = (lax.axis_index("sp"), lax.axis_index("tp"))
+    z, y = (sp // 2, sp % 2)
+    x, c = (tp // 2, tp % 2)
+    peer_c = {"sp": sp, "tp": x * 2 + 1 - c}
+    peer_x = {"sp": sp, "tp": (1 - x) * 2 + c}
+    peer_y = {"sp": z * 2 + 1 - y, "tp": tp}
+
+    def peer_z(k):
+        return {"sp": ((z + k) % depth) * 2 + y, "tp": tp}
+
+    def copy(src, dst, send, recv, peer):
+        return pltpu.make_async_remote_copy(
+            src_ref=src, dst_ref=dst, send_sem=send, recv_sem=recv,
+            device_id=peer, device_id_type=pl.DeviceIdType.MESH,
+        )
+
+    cols_a, cols_b = (pl.ds(0, half), pl.ds(half, wide - half))
+    sum_a, sum_b = (pl.ds(0, half), pl.ds(half, half))
+    every = pl.ds(0, rows)
+
+    def ag(k, n):
+        sems = (g_send.at[k, n], g_recv.at[k, n])
+        if n == 0:
+            return copy(xs.at[k, 0], xs.at[k, DX], *sems, peer_x)
+        if n == 1:
+            return copy(xs.at[k, 0], xs.at[k, DY], *sems, peer_y)
+        if n == 2:
+            return copy(
+                xs.at[k, DX, every, cols_a], xs.at[k, DX + DY, every, cols_a], *sems, peer_y
+            )
+        if n == 3:
+            return copy(
+                xs.at[k, DY, every, cols_b], xs.at[k, DX + DY, every, cols_b], *sems, peer_x
+            )
+        return copy(xs.at[k, n - 4], xs.at[k, DC + n - 4], *sems, peer_c)
+
+    def zg(k):
+        return copy(xs.at[0, 0], xs.at[k, 0], z_send.at[k], z_recv.at[k], peer_z(k))
+
+    def rs(k, n):
+        sems = (r_send.at[k, n], r_recv.at[k, n])
+        if n == 0:
+            return copy(part.at[k, pl.ds(DC, DC)], from_core.at[k], *sems, peer_c)
+        if n == 1:
+            return copy(part.at[k, DY, every, sum_a], from_y.at[k, 0], *sems, peer_y)
+        if n == 2:
+            return copy(part.at[k, DX + DY, every, sum_a], from_y.at[k, 1], *sems, peer_y)
+        if n == 3:
+            return copy(part.at[k, DX, every, sum_b], from_x.at[k, 0], *sems, peer_x)
+        if n == 4:
+            return copy(part.at[k, DX + DY, every, sum_b], from_x.at[k, 1], *sems, peer_x)
+        if n == 5:
+            return copy(part.at[k, DX, every, sum_a], last_x.at[k], *sems, peer_x)
+        return copy(part.at[k, DY, every, sum_b], last_y.at[k], *sems, peer_y)
+
+    def zr(k):
+        return copy(part.at[k, 0], from_z.at[k], e_send.at[k], e_recv.at[k], peer_z(depth - k))
+
+    def added(slot, columns, arrived):
+        k, s = slot
+        now = part[k, s, :, columns].astype(jnp.float32) + arrived.astype(jnp.float32)
+        part[k, s, :, columns] = now.astype(jnp.bfloat16)
+
+    loads = [
+        pltpu.make_async_copy(gate_hbm.at[0], gate_w, load_sem.at[0]),
+        pltpu.make_async_copy(up_hbm.at[0], up_w, load_sem.at[1]),
+        pltpu.make_async_copy(down_hbm.at[0], down_w, load_sem.at[2]),
+    ]
+    own = pltpu.make_async_copy(ext_ref, xs.at[0, 0], load_sem.at[3])
+    own.start()
+    barrier = pltpu.get_barrier_semaphore()
+    peers = [peer_c, peer_x, peer_y] + [peer_z(k) for k in range(1, depth)]
+    for peer in peers:
+        pl.semaphore_signal(barrier, inc=1, device_id=peer, device_id_type=pl.DeviceIdType.MESH)
+    pl.semaphore_wait(barrier, len(peers))
+    own.wait()
+    for n in (0, 1, 4):
+        ag(0, n).start()
+    for k in range(1, depth):
+        zg(k).start()
+    for load in loads:
+        load.start()
+
+    block = 4
+    lane = lax.broadcasted_iota(jnp.int32, (block * rows, LANES), 1)
+    chosen = (lane == sp) | (lane == sp + LANES // 2)
+
+    def compute(k):
+        def chunk(j, none):
+            held = xs[k, pl.ds(j * block, block)].reshape(block * rows, wide)
+            rows_in = held[:, :width]
+            weight = jnp.sum(
+                jnp.where(chosen, held[:, width:].astype(jnp.float32), 0.0), axis=1, keepdims=True
+            )
+            g = jnp.dot(rows_in, gate_w[...], preferred_element_type=jnp.float32)
+            u = jnp.dot(rows_in, up_w[...], preferred_element_type=jnp.float32)
+            act = (clamp_units(g, u) * weight).astype(jnp.bfloat16)
+            down = jnp.dot(act, down_w[...], preferred_element_type=jnp.float32)
+            part[k, pl.ds(j * block, block)] = down.astype(jnp.bfloat16).reshape(
+                block, rows, width
+            )
+            return none
+
+        lax.fori_loop(0, 2, chunk, 0)
+
+    def step(k, none):
+        live, late = (k < depth, k > 0)
+
+        @pl.when(live)
+        def _():
+            ag(k, 0).wait_recv()
+            ag(k, 1).wait_recv()
+            for n in (2, 3, 4 + DX, 4 + DY):
+                ag(k, n).start()
+
+        @pl.when(k + 1 < depth)
+        def _():
+            zg(k + 1).wait_recv()
+            for n in (0, 1, 4):
+                ag(k + 1, n).start()
+
+        @pl.when(late)
+        def _():
+            p = k - 1
+            rs(p, 0).wait_recv()
+            for s in range(DC):
+                added((p, s), slice(0, width), from_core[p, s])
+            for n in (1, 2, 3, 4):
+                rs(p, n).start()
+
+        @pl.when(live)
+        def _():
+            ag(k, 2).wait_recv()
+            ag(k, 3).wait_recv()
+            ag(k, 4 + DX + DY).start()
+
+        @pl.when(late)
+        def _():
+            p = k - 1
+            for n in (1, 2, 3, 4):
+                rs(p, n).wait_recv()
+            added((p, DX), slice(0, half), from_y[p, 1])
+            added((p, DY), slice(half, width), from_x[p, 1])
+            rs(p, 5).start()
+            rs(p, 6).start()
+            added((p, 0), slice(0, half), from_y[p, 0])
+            added((p, 0), slice(half, width), from_x[p, 0])
+
+        @pl.when(k == 0)
+        def _():
+            for load in loads:
+                load.wait()
+
+        @pl.when(live)
+        def _():
+            for n in (4, 5, 6, 7):
+                ag(k, n).wait_recv()
+            compute(k)
+            rs(k, 0).start()
+
+        @pl.when(late)
+        def _():
+            p = k - 1
+            rs(p, 5).wait_recv()
+            rs(p, 6).wait_recv()
+            added((p, 0), slice(0, half), last_x[p])
+            added((p, 0), slice(half, width), last_y[p])
+
+        @pl.when(k > 1)
+        def _():
+            zr(k - 1).start()
+
+        return none
+
+    lax.fori_loop(0, depth + 1, step, 0)
+    total = hid_ref[...].astype(jnp.float32) + part[0, 0].astype(jnp.float32)
+    for k in range(1, depth):
+        zr(k).wait_recv()
+        total = total + from_z[k].astype(jnp.float32)
+    out_ref[...] = total.astype(out_ref.dtype)
+
+    def drain(k, none):
+        for n in range(8):
+            ag(k, n).wait_send()
+        for n in range(7):
+            rs(k, n).wait_send()
+        return none
+
+    lax.fori_loop(0, depth, drain, 0)
+    for k in range(1, depth):
+        zg(k).wait_send()
+        zr(k).wait_send()
+
+
+def experts(ext, hidden, expert_gate, expert_up, expert_down):
+    depth = lax.axis_size("sp") // 2
+    rows, width = hidden.shape
+    wide = ext.shape[1]
+    kind = jnp.bfloat16
+    vmem = pl.BlockSpec(memory_space=pltpu.VMEM)
+    hbm = pl.BlockSpec(memory_space=pl.ANY)
+    half = width // 2
+    dma = pltpu.SemaphoreType.DMA
+    return pl.pallas_call(
+        functools.partial(moe_kernel, depth),
+        out_shape=jax.ShapeDtypeStruct(hidden.shape, kind),
+        in_specs=[vmem, vmem, hbm, hbm, hbm],
+        out_specs=vmem,
+        scratch_shapes=[
+            pltpu.VMEM((depth, 8, rows, wide), kind),
+            pltpu.VMEM((depth, 8, rows, width), kind),
+            pltpu.VMEM((depth, 4, rows, width), kind),
+            pltpu.VMEM((depth, 2, rows, half), kind),
+            pltpu.VMEM((depth, 2, rows, half), kind),
+            pltpu.VMEM((depth, rows, half), kind),
+            pltpu.VMEM((depth, rows, half), kind),
+            pltpu.VMEM((depth, rows, width), kind),
+            pltpu.VMEM(expert_gate.shape[1:], kind),
+            pltpu.VMEM(expert_up.shape[1:], kind),
+            pltpu.VMEM(expert_down.shape[1:], kind),
+            dma((4,)),
+            dma((depth,)),
+            dma((depth,)),
+            dma((depth, 8)),
+            dma((depth, 8)),
+            dma((depth, 7)),
+            dma((depth, 7)),
+            dma((depth,)),
+            dma((depth,)),
+        ],
+        compiler_params=pltpu.CompilerParams(
+            collective_id=1, has_side_effects=True, vmem_limit_bytes=56 * 1024 * 1024
+        ),
+    )(ext, hidden, expert_gate, expert_up, expert_down)
 
 
 def shards(
@@ -110,25 +409,19 @@
     seq_rows, channels = conv_input.shape
     tap_count = conv_taps.shape[0]
     earlier = shifted(conv_input[seq_rows - tap_count + 1 :], "sp", 1)
-    padded = jnp.concatenate([earlier, conv_input], axis=0).astype(jnp.float32)
-    convolved = jnp.zeros((seq_rows, channels), jnp.float32)
-    for offset in range(tap_count):
-        convolved = convolved + padded[offset : offset + seq_rows] * conv_taps[offset]
-    convolved = convolved.astype(jnp.bfloat16)
-    gate_pre = head_maps(convolved, narrow_maps, wide_maps)
-    log_decay = (
-        -DECAY_SCALE * jax.nn.sigmoid(gate_pre[0]) * jax.nn.softplus(-decay_param) + decay_shift
-    )
-    driving = (
-        jnp.sqrt(-jnp.expm1(2.0 * log_decay))
-        * jax.nn.sigmoid(gate_pre[1])
-        * convolved.astype(jnp.float32)
-    )
-    identity = (jnp.ones((channels,), jnp.float32), jnp.zeros((channels,), jnp.float32))
-    factors, local_state = lax.associative_scan(
-        combine_steps, (jnp.exp(log_decay), driving), axis=0
-    )
-    carried = prefix((factors[-1], local_state[-1]), "sp", combine_steps, identity)
+    head = jnp.zeros((SUBLANES, channels), jnp.float32)
+    head = head.at[SUBLANES - tap_count + 1 :].set(earlier.astype(jnp.float32))
+    soft = jax.nn.softplus(-decay_param)[None, :]
+    factors, local_state = mix_local(
+        head, conv_input, conv_taps, narrow_maps, wide_maps, soft, decay_shift
+    )
+    ends = lax.all_gather(jnp.stack([factors[-1], local_state[-1]]), "sp")
+    mine = lax.axis_index("sp")
+    state = jnp.zeros((channels,), jnp.float32)
+    for position in range(lax.axis_size("sp") - 1):
+        longer = ends[position, 0] * state + ends[position, 1]
+        state = jnp.where(position < mine, longer, state)
+    carried = (None, state)
     recurrent = local_state + factors * carried[1]
     gated_rows = (recurrent * jax.nn.gelu(gate_branch.astype(jnp.float32))).astype(jnp.bfloat16)
     tp_count = lax.axis_size("tp")
@@ -154,6 +447,22 @@
     own_index = lax.axis_index("tp")
     assignments = tok_local * top_count
     own_rows = lax.dynamic_slice_in_dim(routes, own_index * tok_local, tok_local, 0)
+    own_weights = lax.dynamic_slice_in_dim(route_weights, own_index * tok_local, tok_local, 0)
+    whole_rows = capacity >= tok_local and expert_gate.shape[0] == 1
+    if whole_rows and tp_count == 4 and lax.axis_size("sp") % 2 == 0:
+        spread = jnp.sum(
+            jnp.where(
+                own_rows[:, :, None] == jnp.arange(LANES // 2, dtype=jnp.int32)[None, None, :],
+                own_weights[:, :, None],
+                0.0,
+            ),
+            axis=1,
+        )
+        high = lax.reduce_precision(spread, exponent_bits=8, mantissa_bits=7)
+        ext = jnp.concatenate(
+            [normed, high.astype(jnp.bfloat16), (spread - high).astype(jnp.bfloat16)], axis=1
+        )
+        return experts(ext, hidden, expert_gate, expert_up, expert_down)
     own_routes = own_rows.reshape(assignments)
     own_ranks = slot_ranks(own_routes[None, :], expert_total)[0]
     source = jnp.arange(assignments, dtype=jnp.int32) // top_count

time: 564 us -> 198 us (0.35); the launches traced: 558 us -> 198 us
  waiting for transfers between devices: 281 us -> 29.7 us
  Pallas kernels: 0 us -> 110 us
  local copies, waits for them, and re-layouts: 84.7 us -> 8.05 us
  blocking collectives: 99.9 us -> 27.9 us
  other arithmetic: 37.6 us -> 2.19 us
  matrix products: 31.2 us -> 2.8 us
  starting transfers between devices: 9.82 us -> 3.42 us
    unnamed x4 -> x1, waiting for transfers between devices: 152 us -> 0.02 us
    pallas_call x0 -> x2, Pallas kernels: none -> 110 us  [the longest x1 109 us: experts(): pl.pallas_call(functools.partial(moe_kernel, depth), out_shape=jax.ShapeD...]
    slice x57 -> x2, local copies, waits for them, and re-layouts: 61.1 us -> 0.01 us  [shards(): ends = lax.all_gather(jnp.stack([factors[-1], local_state[-1]]), 'sp')]
    all_gather x1 -> x0, waiting for transfers between devices: 58.5 us -> none  [shards(): lax.all_gather(lax.all_to_all(outgoing, 'sp', split_axis=0, concat_axis=0...]
    all_to_all x1 -> x0, blocking collectives: 51.3 us -> none  [shards(): lax.all_to_all(outgoing, 'sp', split_axis=0, concat_axis=0, tiled=True)]
    all_to_all x1 -> x0, waiting for transfers between devices: 46.2 us -> none  [shards(): lax.all_to_all(summed, 'sp', split_axis=0, concat_axis=0, tiled=True)]
    dot_general x4 -> x0, matrix products: 27.2 us -> none  [the longest x1 15.3 us: expert_work(): jnp.einsum('sxcf,xfd->sxcd', activation, expert_down, preferred_element_t...]
    all_gather x2 -> x1, blocking collectives: 48.6 us -> 27.9 us  [shards(): ends = lax.all_gather(jnp.stack([factors[-1], local_state[-1]]), 'sp')]
  transfers between devices with their start and end apart: 5 -> 2, of which waited for: 5 -> 2; matrix products, arithmetic and copies ran while one was open for 1% -> 1% of each run, Pallas kernels for 0% -> 0%
where the time goes in v1:
time: 198 us
  Pallas kernels  110 us (56%)
  waiting for transfers between devices  29.7 us (15%)
  blocking collectives  27.9 us (14%)
  between operations  13.6 us (7%)
  local copies, waits for them, and re-layouts  8.05 us (4%)
  starting transfers between devices  3.42 us (2%)
  matrix products  2.8 us (1%)
  other arithmetic  2.19 us (1%)
    pallas_call x1, Pallas kernels, experts(): pl.pallas_call(functools.partial(moe_kernel, depth), out_shape=jax.ShapeD...  109 us
    all_gather x1, blocking collectives, shards(): ends = lax.all_gather(jnp.stack([factors[-1], local_state[-1]]), 'sp')  27.9 us
    reduce_scatter x1, waiting for transfers between devices, shards(): lax.psum_scatter(jnp.dot(gated_rows, mixer_out, preferred_element_type=jn...  27.4 us
    unnamed x23, local copies, waits for them, and re-layouts  6.24 us
  transfers between devices with their start and end apart: 2, of which 2 were waited for; matrix products, arithmetic and copies ran while one was open for 1% of the time, Pallas kernels for 0%

profile of v1, /device:TPU:24, one launch (start us, length us, event | category | flops | bytes accessed | tf_op | source)
XLA Modules:
  0.0 198.0 jit_solution(2881502508361819242)
XLA Ops:
  6.5 0.9 slice.67
  7.4 3.4 %collective-permute-start = (bf16[3,512]{1,0:T(4,128)(2,1)S(1)}, bf16[3,512]{1,0:T(4,128)(2,1)S(1)}, u32[]{:S(2)}, u32[]{:S(2)}) collective-permute-start(bf16[3,512]{1,0:T(4,128)(2,1)S(1)} %slice.67), channel_id=1, source_target_pairs={{0,4},{4,8},{8,12},{12,16},{16,20},{20,24},{24,28},{1,5},{5,9},{9,... | collective-permute-start | bytes 9224 | tf_op jit(solution)/shard_map/ppermute | solution.py:19
  10.8 0.7 compare_select_fusion
  11.5 2.3 %collective-permute-done = bf16[3,512]{1,0:T(4,128)(2,1)S(1)} collective-permute-done((bf16[3,512]{1,0:T(4,128)(2,1)S(1)}, bf16[3,512]{1,0:T(4,128)(2,1)S(1)}, u32[]{:S(2)}, u32[]{:S(2)}) %collective-permute-start) | collective-permute-done | bytes 3104 | tf_op jit(solution)/shard_map/ppermute | solution.py:19
  13.8 1.0 copy-done.1
  14.8 0.9 copy-done.2
  15.8 0.9 copy-done.3
  16.7 0.9 copy-done.4
  17.6 0.7 copy-done.5
  18.3 1.7 shard_map.145
  20.1 27.9 %all-gather.1 = f32[8,2,512]{2,1,0:T(2,128)S(1)} all-gather(f32[1,2,512]{2,1,0:T(2,128)S(1)} %maximum_bitcast_fusion), channel_id=2, replica_groups=mesh['sp'=8,'tp'=4] {'sp'}, dimensions={0}, use_global_device_ids=true | all-gather | bytes 36864 | tf_op jit(solution)/shard_map/all_gather | solution.py:418
  48.1 0.0 copy-start.9
  48.1 0.0 copy-start.10
  48.1 2.8 %convolution_convert_fusion = bf16[256,2048]{1,0:T(8,128)(2,1)} fusion(bf16[512,2048]{1,0:T(8,128)(2,1)S(1)} %copy-done, bf16[256,512]{1,0:T(8,128)(2,1)} %param.18, f32[256,512]{1,0:T(8,128)S(1)} %get-tuple-element.19, f32[256,512]{1,0:T(8,128)S(1)} %get-tuple-element.20, f32[512]{0:T(512)S(1)} %add_select_fusion), kind=kOutput, calls=%fused_computation | convolution fusion | flops 539099136 | bytes 4458496 | tf_op jit(solution)/shard_map/dot_general | solution.py:430
  50.9 0.0 reduce-scatter.2.cloned.1.call-update
  51.0 0.1 constant_dynamic-slice_fusion
  51.1 0.1 constant_dynamic-slice_fusion.1
  51.1 0.1 select_reduce_fusion
  51.3 27.4 %reduce-scatter.2.cloned.1.call-done = bf16[64,2048]{1,0:T(8,128)(2,1)} async-done(((bf16[256,2048]{1,0:T(8,128)(2,1)}), bf16[64,2048]{1,0:T(8,128)(2,1)}) %reduce-scatter.2.cloned.1.call-update) | async-done | bytes 262160 | tf_op jit(solution)/shard_map/reduce_scatter | solution.py:429
  78.7 1.1 fusion
  79.9 0.1 fusion.2
  80.0 0.8 concatenate.5.ext_ref
  80.8 108.6 %shard_map.146 = bf16[64,2048]{1,0:T(8,128)(2,1)} custom-call(bf16[64,2176]{1,0:T(8,128)(2,1)} %concatenate.5.ext_ref, bf16[64,2048]{1,0:T(8,128)(2,1)} %copy-done.6, bf16[1,2048,512]{2,1,0:T(8,128)(2,1)} %gate_hbm.1, bf16[1,2048,512]{2,1,0:T(8,128)(2,1)} %up_hbm.1, bf16[1,512,2048]{2,1,0:T(8,128)(2,1)} %down_hbm.1), custom_call_target="tpu_custom_call" | custom-call | tf_op jit(solution)/shard_map/pallas_call | solution.py:359
  189.4 1.7 copy.21
  (24 shorter events, 0.1 us)
Async XLA Ops:
  6.5 41.6 %copy-start = (bf16[512,2048]{1,0:T(8,128)(2,1)S(1)}, bf16[512,2048]{1,0:T(8,128)(2,1)}, u32[]{:S(2)}) copy-start(bf16[512,2048]{1,0:T(8,128)(2,1)} %param.24) | copy-start | bytes 6291460
  6.5 72.2 %reduce-scatter.2.cloned.1.call-start = ((), (), s32[]{:S(2)}) async-start(), calls=%async_computation.1 | async-start | bytes 1310720 | tf_op jit(solution)/shard_map/reduce_scatter | solution.py:429
  7.4 6.4 %collective-permute-start = (bf16[3,512]{1,0:T(4,128)(2,1)S(1)}, bf16[3,512]{1,0:T(4,128)(2,1)S(1)}, u32[]{:S(2)}, u32[]{:S(2)}) collective-permute-start(bf16[3,512]{1,0:T(4,128)(2,1)S(1)} %slice.67), channel_id=1, source_target_pairs={{0,4},{4,8},{8,12},{12,16},{16,20},{20,24},{24,28},{1,5},{5,9},{9,... | collective-permute-start | bytes 9224 | tf_op jit(solution)/shard_map/ppermute | solution.py:19
  13.8 1.0 copy-start.1
  14.8 0.9 copy-start.2
  15.8 0.9 copy-start.3
  16.7 0.9 copy-start.4
  17.6 0.7 copy-start.5
  48.1 2.9 %copy-start.9 = (f32[256,4]{0,1:T(4,128)S(1)}, f32[256,4]{0,1:T(4,128)}, u32[]{:S(2)}) copy-start(f32[256,4]{0,1:T(4,128)} %param.28) | copy-start | bytes 12292
  48.1 3.0 %copy-start.10 = (s32[256,4]{0,1:T(4,128)S(1)}, s32[256,4]{0,1:T(4,128)}, u32[]{:S(2)}) copy-start(s32[256,4]{0,1:T(4,128)} %param.27) | copy-start | bytes 12292
  48.1 30.6 %copy-start.7 = (bf16[64,2048]{1,0:T(8,128)(2,1)S(1)}, bf16[64,2048]{1,0:T(8,128)(2,1)}, u32[]{:S(2)}) copy-start(bf16[64,2048]{1,0:T(8,128)(2,1)} %param.25) | copy-start | bytes 786436
  48.1 31.7 %copy-start.8 = (f32[2048]{0:T(1024)S(1)}, f32[2048]{0:T(1024)}, u32[]{:S(2)}) copy-start(f32[2048]{0:T(1024)} %param.26) | copy-start | bytes 24580
  79.8 1.0 copy-start.6
Sparse Core Ops, SparseCore 0:
  51.1 27.5 reduce-scatter.1

commit v2 on v1

--- a/solution.py
+++ b/solution.py
@@ -62,6 +62,8 @@
 SUBLANES = 8
 DX, DY, DC = 1, 2, 4
 SERIES_LIMIT = 0.05
+GELU_SCALE = 0.7978845608028654
+GELU_CUBIC = 0.044715
 
 
 def mix_kernel(
@@ -145,6 +147,149 @@
     )(head, conv_input, conv_taps, narrow_maps, wide_maps, soft, decay_shift)
 
 
+def front_kernel(
+    count, conv_ref, gate_ref, taps_ref, narrow_ref, wide_ref, soft_ref, shift_ref, mixer_hbm,
+    stream_ref, gain_ref, spread_ref, hid_ref, ext_ref,
+    head, factor, state, padded, log_keep, drive_keep, halo, ends, gated, mixer, mix, arrived,
+    load_sem, halo_send, halo_recv, end_send, end_recv, mix_send, mix_recv,
+):
+    rows = conv_ref.shape[0]
+    kept, width = stream_ref.shape
+    sp, tp = (lax.axis_index("sp"), lax.axis_index("tp"))
+    x, c = (tp // 2, tp % 2)
+    mesh_id = pl.DeviceIdType.MESH
+
+    def later(k):
+        return {"sp": (sp + k) % count, "tp": tp}
+
+    over_x = {"sp": sp, "tp": (1 - x) * 2 + c}
+    over_both = {"sp": sp, "tp": (1 - x) * 2 + 1 - c}
+    over_c = {"sp": sp, "tp": x * 2 + 1 - c}
+    load = pltpu.make_async_copy(mixer_hbm, mixer, load_sem)
+    load.start()
+    barrier = pltpu.get_barrier_semaphore()
+    peers = [over_x, over_both, over_c] + [later(k) for k in range(1, count)]
+    for peer in peers:
+        pl.semaphore_signal(barrier, inc=1, device_id=peer, device_id_type=mesh_id)
+    pl.semaphore_wait(barrier, len(peers))
+    halo_rows = halo.shape[0]
+    halo_copy = pltpu.make_async_remote_copy(
+        src_ref=conv_ref.at[pl.ds(rows - halo_rows, halo_rows)], dst_ref=halo,
+        send_sem=halo_send, recv_sem=halo_recv, device_id=later(1), device_id_type=mesh_id,
+    )
+    halo_copy.start()
+    halo_copy.wait()
+    before = halo[...].astype(jnp.float32)[halo_rows - SUBLANES :]
+    head[...] = jnp.where(sp > 0, before, jnp.zeros_like(before))
+    mix_kernel(
+        head, conv_ref, taps_ref, narrow_ref, wide_ref, soft_ref, shift_ref,
+        factor, state, padded, log_keep, drive_keep,
+    )
+    ends[0, 0:SUBLANES, :] = factor[rows - SUBLANES :, :]
+    ends[0, SUBLANES:, :] = state[rows - SUBLANES :, :]
+    end_copies = [
+        pltpu.make_async_remote_copy(
+            src_ref=ends.at[0], dst_ref=ends.at[k], send_sem=end_send.at[k],
+            recv_sem=end_recv.at[k], device_id=later(k), device_id_type=mesh_id,
+        )
+        for k in range(1, count)
+    ]
+    for one in end_copies:
+        one.start()
+    g = gate_ref[...].astype(jnp.float32)
+    log_keep[...] = 0.5 * g * (1.0 + jnp.tanh(GELU_SCALE * (g + GELU_CUBIC * g * g * g)))
+    load.wait()
+    for one in end_copies:
+        one.wait()
+    last_factor, last_state = (SUBLANES - 1, 2 * SUBLANES - 1)
+    carry = jnp.zeros((1, conv_ref.shape[1]), jnp.float32)
+    for k in range(count - 1, 0, -1):
+        longer = (
+            ends[k, last_factor : last_factor + 1, :] * carry
+            + ends[k, last_state : last_state + 1, :]
+        )
+        carry = jnp.where(sp >= k, longer, carry)
+    recurrent = state[...] + factor[...] * carry
+    gated[...] = (recurrent * log_keep[...]).astype(jnp.bfloat16)
+
+    def project(chip, slot):
+        some = gated[pl.ds(pl.multiple_of(chip * 2 * kept, 2 * kept), 2 * kept), :]
+        value = jnp.dot(some, mixer[...], preferred_element_type=jnp.float32)
+        mix[slot : slot + 2] = value.astype(jnp.bfloat16).reshape(2, kept, width)
+
+    def give(n, source, peer):
+        return pltpu.make_async_remote_copy(
+            src_ref=mix.at[source], dst_ref=arrived.at[n], send_sem=mix_send.at[n],
+            recv_sem=mix_recv.at[n], device_id=peer, device_id_type=mesh_id,
+        )
+
+    given = [give(0, c, over_x), give(1, 1 - c, over_both), give(2, 3 - c, over_c)]
+    project(1 - x, 0)
+    given[0].start()
+    given[1].start()
+    project(x, 2)
+    given[2].start()
+    total = mix[2 + c].astype(jnp.float32)
+    for n in (2, 0, 1):
+        given[n].wait()
+        total = total + arrived[n].astype(jnp.float32)
+    hidden = (stream_ref[...].astype(jnp.float32) + total).astype(jnp.bfloat16)
+    hid_ref[...] = hidden
+    wide = hidden.astype(jnp.float32)
+    mean = jnp.mean(wide * wide, axis=-1, keepdims=True)
+    normed = wide * lax.rsqrt(mean + NORM_EPSILON) * gain_ref[...]
+    ext_ref[:, :width] = normed.astype(jnp.bfloat16)
+    ext_ref[:, width:] = spread_ref[...]
+
+
+def front(
+    conv_input, gate_branch, conv_taps, narrow_maps, wide_maps, soft, decay_shift, mixer_out,
+    stream, norm_gain, spread,
+):
+    count = lax.axis_size("sp")
+    rows, channels = conv_input.shape
+    kept, width = stream.shape
+    single, kind = (jnp.float32, jnp.bfloat16)
+    vmem = pl.BlockSpec(memory_space=pltpu.VMEM)
+    dma = pltpu.SemaphoreType.DMA
+    return pl.pallas_call(
+        functools.partial(front_kernel, count),
+        out_shape=(
+            jax.ShapeDtypeStruct((kept, width), kind),
+            jax.ShapeDtypeStruct((kept, width + LANES), kind),
+        ),
+        in_specs=[vmem] * 7 + [pl.BlockSpec(memory_space=pl.ANY)] + [vmem] * 3,
+        out_specs=(vmem, vmem),
+        scratch_shapes=[
+            pltpu.VMEM((SUBLANES, channels), single),
+            pltpu.VMEM((rows, channels), single),
+            pltpu.VMEM((rows, channels), single),
+            pltpu.VMEM((rows + SUBLANES, channels), single),
+            pltpu.VMEM((rows, channels), single),
+            pltpu.VMEM((rows, channels), single),
+            pltpu.VMEM((2 * SUBLANES, channels), kind),
+            pltpu.VMEM((count, 2 * SUBLANES, channels), single),
+            pltpu.VMEM((rows, channels), kind),
+            pltpu.VMEM(mixer_out.shape, kind),
+            pltpu.VMEM((4, kept, width), kind),
+            pltpu.VMEM((3, kept, width), kind),
+            dma,
+            dma,
+            dma,
+            dma((count,)),
+            dma((count,)),
+            dma((3,)),
+            dma((3,)),
+        ],
+        compiler_params=pltpu.CompilerParams(
+            collective_id=2, has_side_effects=True, vmem_limit_bytes=40 * 1024 * 1024
+        ),
+    )(
+        conv_input, gate_branch, conv_taps, narrow_maps, wide_maps, soft, decay_shift, mixer_out,
+        stream, norm_gain, spread,
+    )
+
+
 def moe_kernel(
     depth, ext_ref, hid_ref, gate_hbm, up_hbm, down_hbm, out_ref,
     xs, part, from_core, from_y, from_x, last_x, last_y, from_z, gate_w, up_w, down_w,
@@ -241,7 +386,8 @@
     chosen = (lane == sp) | (lane == sp + LANES // 2)
 
     def compute(k):
-        def chunk(j, none):
+        def chunk(i, none):
+            j = 1 - i
             held = xs[k, pl.ds(j * block, block)].reshape(block * rows, wide)
             rows_in = held[:, :width]
             weight = jnp.sum(
@@ -254,6 +400,11 @@
             part[k, pl.ds(j * block, block)] = down.astype(jnp.bfloat16).reshape(
                 block, rows, width
             )
+
+            @pl.when(i == 0)
+            def _():
+                rs(k, 0).start()
+
             return none
 
         lax.fori_loop(0, 2, chunk, 0)
@@ -273,15 +424,6 @@
             zg(k + 1).wait_recv()
             for n in (0, 1, 4):
                 ag(k + 1, n).start()
-
-        @pl.when(late)
-        def _():
-            p = k - 1
-            rs(p, 0).wait_recv()
-            for s in range(DC):
-                added((p, s), slice(0, width), from_core[p, s])
-            for n in (1, 2, 3, 4):
-                rs(p, n).start()
 
         @pl.when(live)
         def _():
@@ -311,7 +453,11 @@
             for n in (4, 5, 6, 7):
                 ag(k, n).wait_recv()
             compute(k)
-            rs(k, 0).start()
+            rs(k, 0).wait_recv()
+            for s in range(DC):
+                added((k, s), slice(0, width), from_core[k, s])
+            for n in (1, 2, 3, 4):
+                rs(k, n).start()
 
         @pl.when(late)
         def _():
@@ -408,10 +554,36 @@
 ):
     seq_rows, channels = conv_input.shape
     tap_count = conv_taps.shape[0]
+    tp_count = lax.axis_size("tp")
+    tok_local = seq_rows // tp_count
+    top_count = routes.shape[1]
+    expert_total = expert_gate.shape[0] * lax.axis_size("sp")
+    capacity = max(2, 2 * tok_local * top_count // expert_total)
+    own_index = lax.axis_index("tp")
+    own_rows = lax.dynamic_slice_in_dim(routes, own_index * tok_local, tok_local, 0)
+    own_weights = lax.dynamic_slice_in_dim(route_weights, own_index * tok_local, tok_local, 0)
+    soft = jax.nn.softplus(-decay_param)[None, :]
+    whole_rows = capacity >= tok_local and expert_gate.shape[0] == 1
+    if whole_rows and tp_count == 4 and lax.axis_size("sp") % 2 == 0:
+        lane = jnp.arange(LANES, dtype=jnp.int32)
+        spread = jnp.sum(
+            jnp.where(
+                own_rows[:, :, None] == (lane % (LANES // 2))[None, None, :],
+                own_weights[:, :, None],
+                0.0,
+            ),
+            axis=1,
+        )
+        high = lax.reduce_precision(spread, exponent_bits=8, mantissa_bits=7)
+        pair = jnp.where(lane[None, :] < LANES // 2, high, spread - high).astype(jnp.bfloat16)
+        hidden, ext = front(
+            conv_input, gate_branch, conv_taps, narrow_maps, wide_maps, soft, decay_shift,
+            mixer_out, stream, norm_gain[None, :], pair,
+        )
+        return experts(ext, hidden, expert_gate, expert_up, expert_down)
     earlier = shifted(conv_input[seq_rows - tap_count + 1 :], "sp", 1)
     head = jnp.zeros((SUBLANES, channels), jnp.float32)
     head = head.at[SUBLANES - tap_count + 1 :].set(earlier.astype(jnp.float32))
-    soft = jax.nn.softplus(-decay_param)[None, :]
     factors, local_state = mix_local(
         head, conv_input, conv_taps, narrow_maps, wide_maps, soft, decay_shift
     )
@@ -424,8 +596,6 @@
     carried = (None, state)
     recurrent = local_state + factors * carried[1]
     gated_rows = (recurrent * jax.nn.gelu(gate_branch.astype(jnp.float32))).astype(jnp.bfloat16)
-    tp_count = lax.axis_size("tp")
-    tok_local = seq_rows // tp_count
     mixer_sum = lax.psum_scatter(
         jnp.dot(gated_rows, mixer_out, preferred_element_type=jnp.float32).astype(jnp.bfloat16),
         "tp",
@@ -441,28 +611,7 @@
         * norm_gain
     ).astype(jnp.bfloat16)
     model_width = normed.shape[1]
-    top_count = routes.shape[1]
-    expert_total = expert_gate.shape[0] * lax.axis_size("sp")
-    capacity = max(2, 2 * tok_local * top_count // expert_total)
-    own_index = lax.axis_index("tp")
     assignments = tok_local * top_count
-    own_rows = lax.dynamic_slice_in_dim(routes, own_index * tok_local, tok_local, 0)
-    own_weights = lax.dynamic_slice_in_dim(route_weights, own_index * tok_local, tok_local, 0)
-    whole_rows = capacity >= tok_local and expert_gate.shape[0] == 1
-    if whole_rows and tp_count == 4 and lax.axis_size("sp") % 2 == 0:
-        spread = jnp.sum(
-            jnp.where(
-                own_rows[:, :, None] == jnp.arange(LANES // 2, dtype=jnp.int32)[None, None, :],
-                own_weights[:, :, None],
-                0.0,
-            ),
-            axis=1,
-        )
-        high = lax.reduce_precision(spread, exponent_bits=8, mantissa_bits=7)
-        ext = jnp.concatenate(
-            [normed, high.astype(jnp.bfloat16), (spread - high).astype(jnp.bfloat16)], axis=1
-        )
-        return experts(ext, hidden, expert_gate, expert_up, expert_down)
     own_routes = own_rows.reshape(assignments)
     own_ranks = slot_ranks(own_routes[None, :], expert_total)[0]
     source = jnp.arange(assignments, dtype=jnp.int32) // top_count
@@ -489,7 +638,6 @@
     returned = lax.all_to_all(summed, "sp", split_axis=0, concat_axis=0, tiled=True)
     own_slots = own_routes * capacity + own_ranks
     picked = returned.reshape(expert_total * capacity, model_width)[own_slots]
-    own_weights = lax.dynamic_slice_in_dim(route_weights, own_index * tok_local, tok_local, 0)
     combined = jnp.sum(
         picked.reshape(tok_local, top_count, model_width).astype(jnp.float32)
         * own_weights[:, :, None],

time: 198 us -> 140 us (0.71)
  waiting for transfers between devices: 29.7 us -> 0 us
  blocking collectives: 27.9 us -> 0 us
  Pallas kernels: 110 us -> 126 us
  between operations: 13.6 us -> 0.06 us
  local copies, waits for them, and re-layouts: 8.05 us -> 12.6 us
  starting transfers between devices: 3.42 us -> 0 us
  matrix products: 2.8 us -> 0 us
    all_gather x1 -> x0, blocking collectives: 27.9 us -> none  [shards(): ends = lax.all_gather(jnp.stack([factors[-1], local_state[-1]]), 'sp')]
    reduce_scatter x1 -> x0, waiting for transfers between devices: 27.4 us -> none  [shards(): lax.psum_scatter(jnp.dot(gated_rows, mixer_out, preferred_element_type=jn...]
    pallas_call x1, Pallas kernels: 1.74 us -> 24.6 us  [front(): pl.pallas_call(functools.partial(front_kernel, count), out_shape=(jax.Sha...]
    pallas_call x1, Pallas kernels: 109 us -> 102 us  [experts(): pl.pallas_call(functools.partial(moe_kernel, depth), out_shape=jax.ShapeD...]
    unnamed x23 -> x25, local copies, waits for them, and re-layouts: 6.24 us -> 11.8 us
    ppermute x1 -> x0, starting transfers between devices: 3.42 us -> none  [shifted(): return lax.ppermute(block, axis, route)]
    dot_general x1 -> x0, matrix products: 2.8 us -> none  [shards(): jnp.dot(gated_rows, mixer_out, preferred_element_type=jnp.float32)]
    ppermute x1 -> x0, waiting for transfers between devices: 2.27 us -> none  [shifted(): return lax.ppermute(block, axis, route)]
  transfers between devices with their start and end apart: 2 -> 0, of which waited for: 2 -> 0; matrix products, arithmetic and copies ran while one was open for 1% -> 0% of each run, Pallas kernels for 0% -> 0%
where the time goes in v2:
time: 140 us
  Pallas kernels  126 us (90%)
  local copies, waits for them, and re-layouts  12.6 us (9%)
    pallas_call x1, Pallas kernels, experts(): pl.pallas_call(functools.partial(moe_kernel, depth), out_shape=jax.ShapeD...  102 us
    pallas_call x1, Pallas kernels, front(): pl.pallas_call(functools.partial(front_kernel, count), out_shape=(jax.Sha...  24.6 us
    unnamed x25, local copies, waits for them, and re-layouts  11.8 us

profile of v2, /device:TPU:24, one launch (start us, length us, event | category | flops | bytes accessed | tf_op | source)
XLA Modules:
  0.0 139.7 jit_solution(907161646541683624)
XLA Ops:
  0.0 0.0 copy-start
  0.0 0.7 compare_select_fusion
  0.7 0.0 copy-done
  0.7 0.1 constant_dynamic-slice_fusion.1
  0.8 0.8 constant_dynamic-slice_fusion
  1.6 0.1 select_reduce_fusion
  1.7 0.0 copy-start.1
  1.7 1.6 %copy-done.1 = bf16[512,2048]{1,0:T(8,128)(2,1)S(1)} copy-done((bf16[512,2048]{1,0:T(8,128)(2,1)S(1)}, bf16[512,2048]{1,0:T(8,128)(2,1)}, u32[]{:S(2)}) %copy-start.1) | copy-done | bytes 2097176
  3.3 0.0 copy-start.2
  3.3 1.0 copy-done.2
  4.3 0.0 copy-start.5
  4.3 0.9 copy-done.5
  5.3 0.9 copy-done.6
  6.2 0.9 copy-done.7
  7.2 0.9 copy-done.8
  8.1 0.9 copy-done.9
  9.1 0.7 copy-done.10
  9.8 0.7 copy-done.11
  10.4 24.6 %shard_map.145 = (bf16[64,2048]{1,0:T(8,128)(2,1)S(1)}, bf16[64,2176]{1,0:T(8,128)(2,1)S(1)}) custom-call(bf16[256,512]{1,0:T(8,128)(2,1)S(1)} %copy-done.5, bf16[256,512]{1,0:T(8,128)(2,1)S(1)} %copy-done.6, f32[4,512]{1,0:T(4,128)S(1)} %copy-done.10, bf16[2,2,128,128]{3,2,1,0:T(8,128)(2,1)S(1)} %copy-done.9, bf16[2,1,256,256]{3,2,1,0:T(8,128)(2,1)S(1)} %copy-done.7, ...), custom_call_target="tpu_custom_call" | custom-call | tf_op jit(solution)/shard_map/pallas_call | solution.py:255
  35.1 0.0 copy-start.3
  35.1 0.7 copy-done.3
  35.8 0.7 copy-done.4
  36.5 101.6 %shard_map.146 = bf16[64,2048]{1,0:T(8,128)(2,1)} custom-call(bf16[64,2176]{1,0:T(8,128)(2,1)} %copy-done.3, bf16[64,2048]{1,0:T(8,128)(2,1)} %copy-done.4, bf16[1,2048,512]{2,1,0:T(8,128)(2,1)} %gate_hbm.1, bf16[1,2048,512]{2,1,0:T(8,128)(2,1)} %up_hbm.1, bf16[1,512,2048]{2,1,0:T(8,128)(2,1)} %down_hbm.1), custom_call_target="tpu_custom_call" | custom-call | tf_op jit(solution)/shard_map/pallas_call | solution.py:505
  138.0 1.7 %copy.19 = bf16[64,2048]{1,0:T(8,128)(2,1)} copy(bf16[64,2048]{1,0:T(8,128)(2,1)} %shard_map.146) | data formatting | bytes 524288
  (10 shorter events, 0.0 us)
Async XLA Ops:
  0.0 0.7 copy-start
  1.7 1.6 %copy-start.1 = (bf16[512,2048]{1,0:T(8,128)(2,1)S(1)}, bf16[512,2048]{1,0:T(8,128)(2,1)}, u32[]{:S(2)}) copy-start(bf16[512,2048]{1,0:T(8,128)(2,1)} %mixer_hbm.1) | copy-start | bytes 6291460
  3.3 1.0 copy-start.2
  4.3 0.9 copy-start.5
  5.3 0.9 copy-start.6
  6.2 0.9 copy-start.7
  7.2 0.9 copy-start.8
  8.1 0.9 copy-start.9
  9.1 0.7 copy-start.10
  9.7 0.7 copy-start.11
  35.1 0.7 copy-start.3
  35.8 0.7 copy-start.4
